TPU v7x, 32 devices: a whole 2x2x4 slice. The times are simulated.
32 devices in a mesh: sp: 16 (over z, y, x), tp: 2 (over core).
Axes of the slice: x: 2, y: 2, z: 4, core: 2. Of those that a mesh axis runs over, the one named last changes fastest.
Arguments:
- block_input: bfloat16 [2048, 2048], P('sp'), may hold values from -6 to 6
- value_weight: bfloat16 [2048, 384], P(None, 'tp'), may hold values from -0.125 to 0.125
- query_pre: bfloat16 [2048, 384], P('sp', 'tp'), may hold values from -6 to 6
- forget_pre: bfloat16 [2048, 384], P('sp', 'tp'), may hold values from -5.5 to 5.5
- lower_bound: float32 [384], P('tp'), may hold values from 0.94 to 1, as said below
- out_grad: bfloat16 [2048, 384], P('sp', 'tp'), may hold values from -6 to 6
Outputs:
- grad_query_pre: bfloat16 [2048, 384], P('sp', 'tp')
- grad_forget_pre: bfloat16 [2048, 384], P('sp', 'tp')
- grad_block_input: bfloat16 [2048, 2048], P(('sp', 'tp'))
- grad_value_weight: float32 [2048, 384], P('sp', 'tp')
Inputs may be any that keep to these rules, and one draw needn't show every extreme that they name: `lower_bound`: each channel's floor is below 1 and at least 0.94.
All inputs are finite; a program needn't handle non-finite values.
Results may differ from a plain program's by a relative error of at most 0.009.
Values may be sent and summed in bfloat16 or wider, within the bound.
A program may use at most 64 MiB of HBM per device.

v0:
```python
import jax
import jax.numpy as jnp
from jax import lax
from jax.sharding import PartitionSpec as P

HEAD = 64
BLOCK = 64


highest = lax.Precision.HIGHEST


def entering(array, axis, combine, identity, reverse):
    size, position = (lax.axis_size(axis), lax.axis_index(axis))
    everything = jax.tree.map(
        lambda part, kind: lax.all_gather(part.astype(kind), axis),
        array,
        (jnp.bfloat16, jnp.bfloat16),
    )
    start = jax.tree.map(
        lambda part, zero: jnp.broadcast_to(jnp.asarray(zero, part.dtype), part.shape),
        array,
        identity,
    )

    def lap(k, before):
        at = size - 1 - k if reverse else k
        reached = at > position if reverse else at < position
        new = combine(
            before, jax.tree.map(lambda part, own: part[at].astype(own.dtype), everything, array)
        )
        return jax.tree.map(lambda a, b: jnp.where(reached, a, b), new, before)

    return lax.fori_loop(0, size, lap, start)


def combine(earlier, latter):
    return (earlier[0] * latter[0], latter[0][..., None] * earlier[1] + latter[1])


def blocked(array, head_count, block_count):
    return jnp.transpose(array.reshape(block_count, BLOCK, head_count, HEAD), (0, 2, 1, 3))


def unblocked(array):
    block_count, head_count = (array.shape[0], array.shape[1])
    return jnp.transpose(array, (0, 2, 1, 3)).reshape(block_count * BLOCK, head_count * HEAD)


def carry_step(carried, pieces):
    decay_b, update_b = pieces
    return (decay_b[..., None] * carried + update_b, carried)


def on_device(block_input, value_weight, query_pre, forget_pre, lower_bound, out_grad):
    token_count = block_input.shape[0]
    group_width = value_weight.shape[1]
    head_count = group_width // HEAD
    block_count = token_count // BLOCK
    value_rows = jnp.dot(block_input, value_weight, preferred_element_type=jnp.float32).astype(
        jnp.bfloat16
    )
    query_f = query_pre.astype(jnp.float32)
    forget_f = forget_pre.astype(jnp.float32)
    query_sig = jax.nn.sigmoid(query_f)
    query = query_f * query_sig
    forget_sig = jax.nn.sigmoid(forget_f)
    key_rate = (1.0 - lower_bound) * jax.nn.sigmoid(-forget_f)
    decay_log = jnp.log1p(-key_rate)
    query_b = blocked(query, head_count, block_count)
    key_b = blocked(key_rate, head_count, block_count)
    value_b = blocked(value_rows.astype(jnp.float32), head_count, block_count)
    decay_b = blocked(decay_log, head_count, block_count)
    grad_b = blocked(out_grad.astype(jnp.float32), head_count, block_count)
    cumulative = jnp.cumsum(decay_b, axis=2)
    closing = cumulative[:, :, -1:, :]
    growth = jnp.exp(cumulative)
    shrinking = jnp.exp(-cumulative)
    remaining = jnp.exp(closing - cumulative)
    query_dec = query_b * growth
    key_dec = key_b * shrinking
    key_end = key_b * remaining
    block_decay = jnp.exp(closing[:, :, 0, :])
    update = jnp.einsum("bhsd,bhsv->bhdv", key_end, value_b, precision=highest)
    reach = jnp.einsum("bhtd,bhtv->bhdv", query_dec, grad_b, precision=highest)
    empty = jnp.zeros((head_count, HEAD, HEAD), jnp.float32)
    unit = jnp.ones((head_count, HEAD), jnp.float32)
    dev_state, starts_local = lax.scan(carry_step, empty, (block_decay, update))
    dev_grad, ends_local = lax.scan(carry_step, empty, (block_decay, reach), reverse=True)
    dev_decay = jnp.prod(block_decay, axis=0)
    running = jnp.cumprod(block_decay, axis=0)
    before = jnp.concatenate([unit[None], running[:-1]], axis=0)
    backward = jnp.flip(jnp.cumprod(jnp.flip(block_decay, 0), axis=0), 0)
    after = jnp.concatenate([backward[1:], unit[None]], axis=0)
    incoming = entering((dev_decay, dev_state), "sp", combine, (unit, empty), False)[1]
    outgoing = entering((dev_decay, dev_grad), "sp", combine, (unit, empty), True)[1]
    starts = starts_local + before[..., None] * incoming[None]
    device_end = dev_decay[..., None] * incoming + dev_state
    ends = jnp.concatenate([starts[1:], device_end[None]], axis=0)
    end_grads = ends_local + after[..., None] * outgoing[None]
    causal = (jnp.arange(BLOCK)[:, None] >= jnp.arange(BLOCK)[None, :]).astype(jnp.float32)
    pairing = jnp.einsum("bhtv,bhsv->bhts", grad_b, value_b, precision=highest) * causal
    mixing = jnp.einsum("bhtd,bhsd->bhts", query_dec, key_dec, precision=highest) * causal
    grad_query = growth * (
        jnp.einsum("bhts,bhsd->bhtd", pairing, key_dec, precision=highest)
        + jnp.einsum("bhdv,bhtv->bhtd", starts, grad_b, precision=highest)
    )
    grad_key = shrinking * jnp.einsum("bhts,bhtd->bhsd", pairing, query_dec, precision=highest)
    grad_key = grad_key + remaining * jnp.einsum(
        "bhdv,bhsv->bhsd", end_grads, value_b, precision=highest
    )
    grad_value = jnp.einsum("bhts,bhtv->bhsv", mixing, grad_b, precision=highest)
    grad_value = grad_value + jnp.einsum("bhsd,bhdv->bhsv", key_end, end_grads, precision=highest)
    boundary = jnp.sum(end_grads * ends, axis=3)
    is_last = (jnp.arange(BLOCK) == BLOCK - 1).astype(jnp.float32)
    grad_cum = (
        query_b * grad_query
        - key_b * grad_key
        + is_last[None, None, :, None] * boundary[:, :, None, :]
    )
    grad_decay = jnp.einsum("ut,bhud->bhtd", causal, grad_cum, precision=highest)
    grad_key_total = grad_key - grad_decay / (1.0 - key_b)
    grad_query_rows = unblocked(grad_query)
    grad_query_pre = grad_query_rows * (query_sig * (1.0 + query_f * (1.0 - query_sig)))
    grad_forget = -unblocked(grad_key_total) * key_rate * forget_sig
    value_grad = unblocked(grad_value).astype(jnp.bfloat16)
    weight_grad = lax.psum_scatter(
        lax.dot_general(
            block_input, value_grad, (((0,), (0,)), ((), ())), preferred_element_type=jnp.float32
        ),
        "sp",
        scatter_dimension=0,
        tiled=True,
    )
    regrouped = lax.all_to_all(value_grad, "tp", split_axis=0, concat_axis=1, tiled=True)
    weight_all = lax.all_gather(value_weight, "tp", axis=1, tiled=True)
    input_grad = jnp.zeros((regrouped.shape[0], weight_all.shape[0]), jnp.float32)
    for member in range(lax.axis_size("tp")):
        lo_col = member * group_width
        partial_value = lax.dot_general(
            regrouped[:, lo_col : lo_col + group_width],
            weight_all[:, lo_col : lo_col + group_width],
            (((1,), (1,)), ((), ())),
            preferred_element_type=jnp.float32,
        )
        partial_value = lax.optimization_barrier(partial_value.astype(jnp.bfloat16))
        input_grad = input_grad + partial_value.astype(jnp.float32)
    return (
        grad_query_pre.astype(jnp.bfloat16),
        grad_forget.astype(jnp.bfloat16),
        input_grad.astype(jnp.bfloat16),
        weight_grad,
    )


def solution(mesh):
    in_specs = (P("sp", None), P(None, "tp"), P("sp", "tp"), P("sp", "tp"), P("tp"), P("sp", "tp"))
    out_specs = (P("sp", "tp"), P("sp", "tp"), P(("sp", "tp"), None), P("sp", "tp"))
    return jax.shard_map(
        on_device, mesh=mesh, in_specs=in_specs, out_specs=out_specs, check_vma=False
    )
```

profile of v0, /device:TPU:0, one launch (start us, length us, event | category | flops | bytes accessed | tf_op | source)
XLA Modules:
  0.0 281.1 jit_solution(12468299078991325864)
XLA Ops:
  8.1 0.7 all-gather.6.cloned.1.call-update
  8.8 0.7 broadcast_subtract_fusion
  9.5 0.9 fusion.23
  10.4 0.2 reshape.97
  10.6 0.1 copy.46
  10.7 0.2 reduce_window_sum.11
  11.1 0.1 copy.48
  11.3 0.4 convolution_convert_fusion.2
  11.7 0.1 copy.47
  11.9 0.2 reshape.100
  12.1 0.1 copy.50
  12.3 0.2 fusion.6
  12.5 0.5 fusion.53
  13.0 0.3 fusion.43
  13.3 0.3 while.60
  13.7 42.5 %all-gather.3 = bf16[16,3,64]{2,1,0:T(4,128)(2,1)S(1)} all-gather(bf16[1,3,64]{2,1,0:T(4,128)(2,1)S(1)} %convert_bitcast_fusion), channel_id=2, replica_groups=mesh['sp'=16,'tp'=2] {'sp'}, dimensions={0}, use_global_device_ids=true | all-gather | bytes 6528 | tf_op jit(solution)/shard_map/all_gather | solution.py:16
  56.2 40.5 %all-gather.1 = bf16[48,64,64]{2,1,0:T(8,128)(2,1)S(1)} all-gather(bf16[3,64,64]{2,1,0:T(8,128)(2,1)S(1)} %convert_element_type.141), channel_id=3, replica_groups=mesh['sp'=16,'tp'=2] {'sp'}, dimensions={0}, use_global_device_ids=true | all-gather | bytes 417792 | tf_op jit(solution)/shard_map/all_gather | solution.py:16
  96.7 2.5 while.61
  96.7 0.1 fusion.71
  96.9 0.1 fusion.71
  97.0 0.1 fusion.71
  97.2 0.1 fusion.71
  97.4 0.1 fusion.71
  97.5 0.1 fusion.71
  97.8 0.1 fusion.71
  98.3 0.1 fusion.71
  99.1 0.1 fusion.71
  99.3 0.1 multiply_add_fusion.1
  99.4 1.0 fusion.18
  100.4 0.1 copy.58
  100.5 0.2 reshape.101
  100.7 0.7 convert_multiply_fusion
  101.4 0.2 reshape.102
  101.5 0.1 copy.59
  101.7 0.3 fusion.37
  102.0 0.3 while.62
  102.4 42.9 %all-gather.2 = bf16[48,64,64]{2,1,0:T(8,128)(2,1)S(1)} all-gather(bf16[3,64,64]{2,1,0:T(8,128)(2,1)S(1)} %convert_element_type.144), channel_id=4, replica_groups=mesh['sp'=16,'tp'=2] {'sp'}, dimensions={0}, use_global_device_ids=true | all-gather | bytes 417792 | tf_op jit(solution)/shard_map/all_gather | solution.py:16
  145.3 2.6 while.63
  145.6 0.1 fusion.72
  146.0 0.1 fusion.72
  146.3 0.1 fusion.72
  146.6 0.1 fusion.72
  146.9 0.1 fusion.72
  147.3 0.1 fusion.72
  147.8 0.1 fusion.72
  148.1 0.5 convolution_multiply_fusion
  148.5 0.2 fusion.35
  148.8 0.4 fusion.8
  149.2 0.1 copy.72
  149.4 1.5 convolution_bitcast_fusion
  150.9 0.1 copy.69
  151.1 0.7 copy.70
  151.8 3.3 %all-to-all-start = ((bf16[2,64,192]{2,1,0:T(8,128)(2,1)}), bf16[2,64,192]{2,1,0:T(8,128)(2,1)S(1)}, u32[]{:S(2)}, u32[]{:S(2)}) async-start(bf16[2,64,192]{2,1,0:T(8,128)(2,1)} %copy.70), calls=%async_computation | async-start | bytes 131072 | tf_op jit(solution)/shard_map/all_to_all | solution.py:135
  155.2 0.2 fusion.11
  155.4 0.3 convolution_multiply_fusion.2
  155.8 0.4 fusion.2
  156.2 0.3 fusion.5
  156.5 0.1 copy.67
  156.7 0.2 neg.26
  157.0 0.7 fusion.52
  157.7 1.4 convolution_convert_fusion
  159.2 1.4 convolution_convert_fusion.1
  160.6 0.8 add_convert_fusion
  161.3 112.3 %reduce-scatter.2.cloned.1.call-done = f32[128,192]{0,1:T(8,128)} async-done(((f32[2048,192]{0,1:T(8,128)}), f32[128,192]{0,1:T(8,128)}) %reduce-scatter.2.cloned.1.call-update) | async-done | bytes 98320 | tf_op jit(solution)/shard_map/reduce_scatter | solution.py:127
  (111 shorter events, 3.7 us)
Async XLA Ops:
  8.0 3.3 %copy-start = (bf16[128,2048]{1,0:T(8,128)(2,1)S(1)}, bf16[128,2048]{1,0:T(8,128)(2,1)}, u32[]{:S(2)}) copy-start(bf16[128,2048]{1,0:T(8,128)(2,1)} %param.14) | copy-start | bytes 1572868
  8.0 3.2 %copy-start.1 = (bf16[2048,192]{0,1:T(8,128)(2,1)S(1)}, bf16[2048,192]{0,1:T(8,128)(2,1)}, u32[]{:S(2)}) copy-start(bf16[2048,192]{0,1:T(8,128)(2,1)} %param.15) | copy-start | bytes 2359300
  8.0 3.0 %copy-start.5 = (bf16[128,192]{0,1:T(8,128)(2,1)S(1)}, bf16[128,192]{0,1:T(8,128)(2,1)}, u32[]{:S(2)}) copy-start(bf16[128,192]{0,1:T(8,128)(2,1)} %param.19) | copy-start | bytes 147460
  8.0 149.7 %all-gather.6.cloned.1.call-start = ((), (), s32[]{:S(2)}) async-start(), calls=%async_computation.2 | async-start | bytes 2359296 | tf_op jit(solution)/shard_map/all_gather | solution.py:136
  8.8 264.9 %reduce-scatter.2.cloned.1.call-start = ((), (), s32[]{:S(2)}) async-start(), calls=%async_computation.3 | async-start | bytes 1671168 | tf_op jit(solution)/shard_map/reduce_scatter | solution.py:127
  96.7 4.0 %copy-start.4 = (bf16[128,192]{0,1:T(8,128)(2,1)S(1)}, bf16[128,192]{0,1:T(8,128)(2,1)}, u32[]{:S(2)}) copy-start(bf16[128,192]{0,1:T(8,128)(2,1)} %param.16) | copy-start | bytes 147460
  102.4 45.6 %copy-start.6 = (pred[2]{0:T(512)(128)(4,1)S(1)}, pred[2]{0:T(512)(128)(4,1)}, u32[]{:S(2)}) copy-start(pred[2]{0:T(512)(128)(4,1)} %constant.137.clone.1) | copy-start | bytes 10
  151.1 5.1 %copy-start.2 = (f32[2,3,64,64]{2,3,1,0:T(8,128)S(1)}, f32[2,3,64,64]{2,3,1,0:T(8,128)}, u32[]{:S(2)}) copy-start(f32[2,3,64,64]{2,3,1,0:T(8,128)} %get-tuple-element.507) | copy-start | bytes 294916
  151.8 5.0 %all-to-all-start = ((bf16[2,64,192]{2,1,0:T(8,128)(2,1)}), bf16[2,64,192]{2,1,0:T(8,128)(2,1)S(1)}, u32[]{:S(2)}, u32[]{:S(2)}) async-start(bf16[2,64,192]{2,1,0:T(8,128)(2,1)} %copy.70), calls=%async_computation | async-start | bytes 131072 | tf_op jit(solution)/shard_map/all_to_all | solution.py:135
  155.8 1.2 copy-start.3
Sparse Core Ops, SparseCore 0:
  10.4 12.5 all-gather.5
Sparse Core Ops, SparseCore 1:
  151.0 122.5 reduce-scatter.1
where the time goes:
time: 281 us
  blocking collectives  126 us (45%)
  waiting for transfers between devices  113 us (40%)
  between operations  15.9 us (6%)
  matrix products  9.16 us (3%)
  other arithmetic  8.93 us (3%)
  local copies, waits for them, and re-layouts  3.39 us (1%)
  starting transfers between devices  3.38 us (1%)
    all_gather x3, blocking collectives, entering(): lax.all_gather(part.astype(kind), axis)  126 us
    reduce_scatter x1, waiting for transfers between devices, on_device(): lax.psum_scatter(lax.dot_general(block_input, value_grad, (((0,), (0,)),...  112 us
  transfers between devices with their start and end apart: 3, of which 1 were waited for; matrix products, arithmetic and copies ran while one was open for 8% of the time, Pallas kernels for 0%

commit v1 on v0

v1 whole, which is shorter than its diff:
```python
import functools

import jax
import jax.numpy as jnp
from jax import lax
from jax.experimental import pallas as pl
from jax.experimental.pallas import tpu as pltpu
from jax.sharding import PartitionSpec as P

HEAD = 64
MESH = pl.DeviceIdType.MESH
f32, bf16 = jnp.float32, jnp.bfloat16
LOGROWS = 16


def nn(a, b):
    return lax.dot_general(a, b, (((1,), (0,)), ((), ())), preferred_element_type=f32)


def nt(a, b):
    return lax.dot_general(a, b, (((1,), (1,)), ((), ())), preferred_element_type=f32)


def tn(a, b):
    return lax.dot_general(a, b, (((0,), (0,)), ((), ())), preferred_element_type=f32)


def split(a):
    high = a.astype(bf16)
    return high, (a - high.astype(f32)).astype(bf16)


def kernel(
    n, n_tp, part,
    x_ref, w_ref, q_ref, f_ref, lb_ref, g_ref,
    gq_ref, gf_ref, gx_ref, gw_ref,
    w_all, xt, xg, smsg, sbuf, dvg, dvp,
    w_send, w_recv, x_send, x_recv, r_send, r_recv, s_send, s_recv,
    d_send, d_recv, p_send, p_recv,
):
    me, core = lax.axis_index("sp"), lax.axis_index("tp")
    tokens, depth = x_ref.shape
    width = q_ref.shape[1]
    heads = width // HEAD
    rows = depth // n
    piece = rows // part
    half = tokens // n_tp

    barrier = pltpu.get_barrier_semaphore()
    for k in range(1, n):
        pl.semaphore_signal(
            barrier, inc=1, device_id=(lax.rem(me + k, n), core), device_id_type=MESH
        )
    for k in range(1, n_tp):
        pl.semaphore_signal(
            barrier, inc=1, device_id=(me, lax.rem(core + k, n_tp)), device_id_type=MESH
        )
    pl.semaphore_wait(barrier, n - 1 + n_tp - 1)

    def mate(k):
        return (me, lax.rem(core + k, n_tp))

    def peer(k):
        return (lax.rem(me + k, n), core)

    def copy_w(k):
        return pltpu.make_async_remote_copy(
            w_ref, w_all.at[k - 1], w_send.at[k - 1], w_recv.at[k - 1], mate(k), MESH
        )

    lead = core * (part - 1)

    def copy_x(k):
        start = pl.multiple_of(lax.rem(me + k, n) * rows + lead * piece, piece)
        lanes = pl.ds(pl.multiple_of(me * tokens, tokens), tokens)
        return pltpu.make_async_remote_copy(
            xt.at[pl.ds(start, piece), :],
            xg.at[lead, :, lanes],
            x_send.at[k - 1], x_recv.at[k - 1], peer(k), MESH,
        )

    def copy_r():
        return pltpu.make_async_remote_copy(
            xg.at[lead], xg.at[lead], r_send.at[0], r_recv.at[0], mate(1), MESH
        )

    def copy_s(k, src):
        return pltpu.make_async_remote_copy(
            smsg.at[(me + k) // n], sbuf.at[src], s_send.at[k - 1], s_recv.at[k - 1], peer(k), MESH
        )

    def copy_d(k):
        mine = dvg.at[pl.ds(pl.multiple_of(me * tokens, tokens), tokens), :]
        return pltpu.make_async_remote_copy(
            mine, mine, d_send.at[k - 1], d_recv.at[k - 1], peer(k), MESH
        )

    def copy_p(k):
        other = lax.rem(core + k, n_tp)
        start = pl.multiple_of(me * tokens + other * half, half)
        return pltpu.make_async_remote_copy(
            dvg.at[pl.ds(start, half), :], dvp.at[k - 1],
            p_send.at[k - 1], p_recv.at[k - 1], mate(k), MESH,
        )

    t_at = lax.broadcasted_iota(jnp.int32, (tokens, tokens), 0)
    s_at = lax.broadcasted_iota(jnp.int32, (tokens, tokens), 1)
    lower = t_at >= s_at
    upper = t_at <= s_at
    lower_b = lower.astype(f32).astype(bf16)
    upper_b = upper.astype(f32).astype(bf16)
    lane_head = lax.broadcasted_iota(jnp.int32, (1, width), 1) // HEAD
    masks = [(lane_head == h).astype(f32) for h in range(heads)]
    masks_b = [m.astype(bf16) for m in masks]

    def stacked(a):
        return jnp.concatenate([a * m for m in masks_b], axis=0)

    def diagonal(full):
        return sum(full[h * HEAD : (h + 1) * HEAD, :] * masks[h] for h in range(heads))

    q_in = q_ref[...].astype(f32)
    f_in = f_ref[...].astype(f32)
    lb = lb_ref[...]
    q_sig = jax.nn.sigmoid(q_in)
    query = q_in * q_sig
    f_sig = jax.nn.sigmoid(f_in)
    key = (1.0 - lb) * jax.nn.sigmoid(-f_in)
    high, low = split(jnp.log1p(-key))
    cumulative = nn(lower_b, high) + nn(lower_b, low)
    closing = cumulative[tokens - 1 : tokens, :]
    growth = jnp.exp(cumulative)
    shrinking = jnp.exp(-cumulative)
    remaining = jnp.exp(closing - cumulative)
    q_dec = (query * growth).astype(bf16)
    k_dec = (key * shrinking).astype(bf16)
    k_end = (key * remaining).astype(bf16)
    g = g_ref[...]
    reach = diagonal(tn(g, q_dec))
    value = nn(x_ref[...], w_ref[...]).astype(bf16)
    update = diagonal(tn(value, k_end))
    log_high, log_low = split(closing)
    row_at = lax.broadcasted_iota(jnp.int32, (LOGROWS, width), 0)
    logs = jnp.where(row_at == 0, log_high.astype(f32), log_low.astype(f32)).astype(bf16)
    for way, part_state in ((0, update), (1, reach)):
        smsg[way, 0:HEAD, :] = part_state.astype(bf16)
        smsg[way, HEAD : HEAD + LOGROWS, :] = logs
    for k in range(1, n):
        copy_s(k, me).start()
    for k in range(1, n_tp):
        copy_w(k).start()
    xt[...] = x_ref[...].T
    for k in range(1, n):
        copy_x(k).start()
    start = pl.multiple_of(me * rows + lead * piece, piece)
    xg[lead, :, pl.ds(pl.multiple_of(me * tokens, tokens), tokens)] = xt[pl.ds(start, piece), :]

    g3, q3, k3, v3 = stacked(g), stacked(q_dec), stacked(k_dec), stacked(value)
    upper3 = jnp.concatenate([upper] * heads, axis=1)
    lower3 = jnp.concatenate([lower] * heads, axis=1)
    mixing_t = jnp.where(upper3, nt(k_dec, q3), 0.0).astype(bf16)
    gv_local = nn(mixing_t, g3)
    pairing_t = jnp.where(upper3, nt(value, g3), 0.0).astype(bf16)
    gk_local = nn(pairing_t, q3)
    pairing = jnp.where(lower3, nt(g, v3), 0.0).astype(bf16)
    gq_local = nn(pairing, k3)

    empty = jnp.zeros((HEAD, width), f32)
    none = jnp.zeros((1, width), f32)

    def take(b, k, carried):
        total, weight_log = carried
        copy_s(k, b).wait_recv()
        total = total + jnp.exp(weight_log) * sbuf[b, 0:HEAD, :].astype(f32)
        tail = sbuf[b, HEAD : HEAD + LOGROWS, :].astype(f32)
        return total, weight_log + tail[0:1, :] + tail[1:2, :]

    outgoing, _ = lax.fori_loop(
        0, n - 1 - me, lambda i, c: take(me + 1 + i, n - 1 - i, c), (empty, none)
    )
    out_b = stacked(outgoing.astype(bf16))
    grad_value = gv_local + nt(k_end, out_b)
    value_grad = grad_value.astype(bf16)
    own = pl.ds(pl.multiple_of(me * tokens, tokens), tokens)
    dvg[own, :] = value_grad
    for k in range(1, n_tp):
        copy_p(k).start()
    for k in range(1, n):
        copy_d(k).start()
    incoming, _ = lax.fori_loop(0, me, lambda i, c: take(me - 1 - i, i + 1, c), (empty, none))

    in_b = stacked(incoming.astype(bf16))
    grad_query = growth * (gq_local + nn(g, in_b))
    grad_key = shrinking * gk_local + remaining * nn(value, out_b)
    ends = jnp.exp(closing) * incoming + update
    boundary = jnp.sum(outgoing * ends, axis=0, keepdims=True)
    c_high, c_low = split(query * grad_query - key * grad_key)
    grad_decay = nn(upper_b, c_high) + nn(upper_b, c_low) + boundary
    gq_ref[...] = (grad_query * (q_sig * (1.0 + q_in * (1.0 - q_sig)))).astype(bf16)
    gf_ref[...] = (-(grad_key - grad_decay / (1.0 - key)) * key * f_sig).astype(bf16)

    for k in range(1, n):
        copy_x(k).wait_recv()
    if part > 1:
        copy_r().start()

    half_rows = pl.ds(pl.multiple_of(me * tokens + core * half, half), half)
    gx = nt(dvg[half_rows, :], w_ref[...]).astype(bf16).astype(f32)
    for k in range(1, n_tp):
        copy_w(k).wait_recv()
        copy_p(k).wait_recv()
        gx = gx + nt(dvp[k - 1], w_all[k - 1]).astype(bf16).astype(f32)
    gx_ref[...] = gx.astype(bf16)

    if part > 1:
        pltpu.make_async_remote_copy(
            xg.at[1 - lead], xg.at[1 - lead], r_send.at[0], r_recv.at[0], mate(1), MESH
        ).wait_recv()
    for k in range(1, n):
        pltpu.make_async_remote_copy(
            dvg.at[own, :],
            dvg.at[pl.ds(pl.multiple_of(lax.rem(me + n - k, n) * tokens, tokens), tokens), :],
            d_send.at[k - 1], d_recv.at[k - 1], peer(k), MESH,
        ).wait_recv()
    for p in range(part):
        gw_ref[pl.ds(p * piece, piece), :] = nn(xg[p], dvg[...])

    for k in range(1, n_tp):
        copy_w(k).wait_send()
        copy_p(k).wait_send()
    if part > 1:
        copy_r().wait_send()
    for k in range(1, n):
        copy_s(k, me).wait_send()
        copy_x(k).wait_send()
        copy_d(k).wait_send()


def on_device(n, n_tp, block_input, value_weight, query_pre, forget_pre, lower_bound, out_grad):
    tokens, depth = block_input.shape
    width = query_pre.shape[1]
    rows = depth // n
    part = 2 if n_tp == 2 and rows % 32 == 0 else 1
    dma = pltpu.SemaphoreType.DMA
    vmem = pl.BlockSpec(memory_space=pltpu.VMEM)
    return pl.pallas_call(
        functools.partial(kernel, n, n_tp, part),
        out_shape=(
            jax.ShapeDtypeStruct((tokens, width), bf16),
            jax.ShapeDtypeStruct((tokens, width), bf16),
            jax.ShapeDtypeStruct((tokens // n_tp, depth), bf16),
            jax.ShapeDtypeStruct((rows, width), f32),
        ),
        in_specs=[vmem] * 6,
        out_specs=(vmem,) * 4,
        scratch_shapes=[
            pltpu.VMEM((n_tp - 1, depth, width), bf16),
            pltpu.VMEM((depth, tokens), bf16),
            pltpu.VMEM((part, rows // part, n * tokens), bf16),
            pltpu.VMEM((2, HEAD + LOGROWS, width), bf16),
            pltpu.VMEM((n, HEAD + LOGROWS, width), bf16),
            pltpu.VMEM((n * tokens, width), bf16),
            pltpu.VMEM((n_tp - 1, tokens // n_tp, width), bf16),
            dma((n_tp - 1,)), dma((n_tp - 1,)),
            dma((n - 1,)), dma((n - 1,)),
            dma((1,)), dma((1,)),
            dma((n - 1,)), dma((n - 1,)),
            dma((n - 1,)), dma((n - 1,)),
            dma((n_tp - 1,)), dma((n_tp - 1,)),
        ],
        compiler_params=pltpu.CompilerParams(
            collective_id=0, has_side_effects=True, vmem_limit_bytes=60 * 1024 * 1024
        ),
    )(block_input, value_weight, query_pre, forget_pre, lower_bound[None, :], out_grad)


def solution(mesh):
    n, n_tp = mesh.shape["sp"], mesh.shape["tp"]
    in_specs = (P("sp", None), P(None, "tp"), P("sp", "tp"), P("sp", "tp"), P("tp"), P("sp", "tp"))
    out_specs = (P("sp", "tp"), P("sp", "tp"), P(("sp", "tp"), None), P("sp", "tp"))
    return jax.shard_map(
        functools.partial(on_device, n, n_tp),
        mesh=mesh, in_specs=in_specs, out_specs=out_specs, check_vma=False,
    )
```

time: 281 us -> 65.1 us (0.23)
  the two profiles are of different devices: /device:TPU:0 before, /device:TPU:30 now
where the time goes in v1:
time: 65.1 us; the launch traced here: 64.7 us
  Pallas kernels  53.3 us (82%)
  local copies, waits for them, and re-layouts  10.8 us (17%)
  between operations  0.66 us (1%)
    pallas_call x1, Pallas kernels, on_device(): pl.pallas_call(functools.partial(kernel, n, n_tp, part), out_shape=(jax.S...  53.3 us
    unnamed x11, local copies, waits for them, and re-layouts  5.98 us
    pallas_call x3, local copies, waits for them, and re-layouts, on_device(): pl.pallas_call(functools.partial(kernel, n, n_tp, part), out_shape=(jax.S...  4.81 us

profile of v1, /device:TPU:30, one launch (start us, length us, event | category | flops | bytes accessed | tf_op | source)
XLA Modules:
  0.0 64.7 jit_solution(5576451399110576001)
XLA Ops:
  0.6 0.0 copy-start.1
  0.6 1.5 %copy.11.q_ref = bf16[128,192]{1,0:T(8,128)(2,1)} copy(bf16[128,192]{0,1:T(8,128)(2,1)} %param.8) | data formatting | bytes 98304 | tf_op args[2]
  2.2 0.0 copy-done.1
  2.2 0.0 copy-start.2
  2.2 0.7 %copy.12.f_ref = bf16[128,192]{1,0:T(8,128)(2,1)} copy(bf16[128,192]{0,1:T(8,128)(2,1)S(1)} %copy-done.1) | data formatting | bytes 98304 | tf_op args[3]
  2.9 0.1 copy-done.2
  3.0 0.7 %copy.13.g_ref = bf16[128,192]{1,0:T(8,128)(2,1)} copy(bf16[128,192]{0,1:T(8,128)(2,1)S(1)} %copy-done.2) | data formatting | bytes 98304 | tf_op args[5]
  3.7 2.2 %copy.10.w_ref = bf16[2048,192]{1,0:T(8,128)(2,1)} copy(bf16[2048,192]{0,1:T(8,128)(2,1)} %param.7) | data formatting | bytes 1572864 | tf_op args[1]
  5.9 53.3 %shard_map.93 = (bf16[128,192]{1,0:T(8,128)(2,1)}, bf16[128,192]{1,0:T(8,128)(2,1)}, bf16[64,2048]{1,0:T(8,128)(2,1)}, f32[128,192]{1,0:T(8,128)}) custom-call(bf16[128,2048]{1,0:T(8,128)(2,1)} %x_ref.1, bf16[2048,192]{1,0:T(8,128)(2,1)} %copy.10.w_ref, bf16[128,192]{1,0:T(8,128)(2,1)} %copy.11.q_ref, bf16[128,192]{1,0:T(8,128)(2,1)} %copy.12.f_ref, ...), custom_call_target="tpu_custom_call" | custom-call | tf_op jit(solution)/shard_map/pallas_call | solution.py:246
  59.2 0.0 copy-start
  59.2 1.6 %copy.14 = bf16[128,192]{0,1:T(8,128)(2,1)} copy(bf16[128,192]{1,0:T(8,128)(2,1)} %get-tuple-element.4) | data formatting | bytes 98304 | tf_op jit(solution)/shard_map/pallas_call | solution.py:246
  60.8 1.6 %copy.15 = bf16[128,192]{0,1:T(8,128)(2,1)} copy(bf16[128,192]{1,0:T(8,128)(2,1)} %get-tuple-element.5) | data formatting | bytes 98304 | tf_op jit(solution)/shard_map/pallas_call | solution.py:246
  62.4 1.6 %copy.16 = f32[128,192]{0,1:T(8,128)} copy(f32[128,192]{1,0:T(8,128)} %get-tuple-element.7) | data formatting | bytes 196608 | tf_op jit(solution)/shard_map/pallas_call | solution.py:246
  64.0 0.0 copy-done
  64.0 0.7 %copy.18 = bf16[64,2048]{1,0:T(8,128)(2,1)} copy(bf16[64,2048]{1,0:T(8,128)(2,1)S(1)} %copy-done) | data formatting | bytes 524288
Async XLA Ops:
  0.6 1.6 %copy-start.1 = (bf16[128,192]{0,1:T(8,128)(2,1)S(1)}, bf16[128,192]{0,1:T(8,128)(2,1)}, u32[]{:S(2)}) copy-start(bf16[128,192]{0,1:T(8,128)(2,1)} %param.9) | copy-start | bytes 147460
  2.2 0.8 %copy-start.2 = (bf16[128,192]{0,1:T(8,128)(2,1)S(1)}, bf16[128,192]{0,1:T(8,128)(2,1)}, u32[]{:S(2)}) copy-start(bf16[128,192]{0,1:T(8,128)(2,1)} %param.11) | copy-start | bytes 147460
  59.2 4.8 %copy-start = (bf16[64,2048]{1,0:T(8,128)(2,1)S(1)}, bf16[64,2048]{1,0:T(8,128)(2,1)}, u32[]{:S(2)}) copy-start(bf16[64,2048]{1,0:T(8,128)(2,1)} %get-tuple-element.14) | copy-start | bytes 786436

commit v2 on v1

v2 whole, which is shorter than its diff:
```python
import functools

import jax
import jax.numpy as jnp
from jax import lax
from jax.experimental import pallas as pl
from jax.experimental.pallas import tpu as pltpu
from jax.sharding import PartitionSpec as P

HEAD = 64
MESH = pl.DeviceIdType.MESH
f32, bf16 = jnp.float32, jnp.bfloat16
LOGROWS = 16


def nn(a, b):
    return lax.dot_general(a, b, (((1,), (0,)), ((), ())), preferred_element_type=f32)


def nt(a, b):
    return lax.dot_general(a, b, (((1,), (1,)), ((), ())), preferred_element_type=f32)


def tn(a, b):
    return lax.dot_general(a, b, (((0,), (0,)), ((), ())), preferred_element_type=f32)


def split(a):
    high = a.astype(bf16)
    return high, (a - high.astype(f32)).astype(bf16)


def kernel(
    inner, outer, n_tp, part,
    x_ref, w_ref, q_ref, f_ref, lb_ref, g_ref,
    gq_ref, gf_ref, gx_ref, gw_ref,
    w_all, xt, xg, b1, f1, bmsg, fmsg, b2, f2, gvk, dvp, dvm, pmsg, pin, dvs,
    w_send, w_recv, x_send, x_recv, r_send, r_recv, b1_send, b1_recv, f1_send, f1_recv,
    b2_send, b2_recv, f2_send, f2_recv, k_send, k_recv, m_send, m_recv, p_send, p_recv,
):
    me, core = lax.axis_index("sp"), lax.axis_index("tp")
    here, plane = lax.rem(me, inner), me // inner
    tokens, depth = x_ref.shape
    width = q_ref.shape[0]
    heads = width // HEAD
    half = tokens // n_tp
    pairs, odd = heads // 2, heads % 2
    wide = 2 * HEAD
    packed = pairs * HEAD + odd * HEAD // 2

    def near(k):
        return (plane * inner + lax.rem(here + k, inner), core)

    def column(k):
        return (lax.rem(plane + k, outer) * inner + here, core)

    def mate(k):
        return (me, lax.rem(core + k, n_tp))

    def rc(src, dst, send, recv, k, to):
        return pltpu.make_async_remote_copy(src, dst, send.at[k - 1], recv.at[k - 1], to, MESH)

    barrier = pltpu.get_barrier_semaphore()
    for to, count in ((near, inner), (column, outer), (mate, n_tp)):
        for k in range(1, count):
            pl.semaphore_signal(barrier, inc=1, device_id=to(k), device_id_type=MESH)

    lead = core * (part - 1)
    own_lanes = pl.ds(pl.multiple_of(here * tokens, tokens), tokens)

    def copy_w(k):
        return rc(w_ref, w_all.at[k - 1], w_send, w_recv, k, mate(k))

    def copy_x(k):
        return rc(
            xt.at[:, lax.rem(here + k, inner), lead], xg.at[:, lead, :, own_lanes],
            x_send, x_recv, k, near(k),
        )

    def copy_r(lane):
        return rc(xg.at[:, lane], xg.at[:, lane], r_send, r_recv, 1, mate(1))

    def copy_b1(k, at):
        return rc(b1.at[at], b1.at[at], b1_send, b1_recv, k, near(k))

    def copy_f1(k, at):
        return rc(f1.at[at], f1.at[at], f1_send, f1_recv, k, near(k))

    def copy_k(k, at):
        return rc(gvk.at[at], gvk.at[at], k_send, k_recv, k, near(k))

    def copy_b2(k, at):
        return rc(bmsg, b2.at[at], b2_send, b2_recv, k, column(k))

    def copy_f2(k, at):
        return rc(fmsg, f2.at[at], f2_send, f2_recv, k, column(k))

    def copy_m(k):
        return rc(dvp.at[:, own_lanes], dvm.at[k - 1], m_send, m_recv, k, mate(k))

    def copy_p(k):
        return rc(pmsg.at[lax.rem(plane + k, outer)], pin.at[k - 1], p_send, p_recv, k, column(k))

    def source(k):
        return lax.rem(here + inner - k, inner)

    lane_low = lax.broadcasted_iota(jnp.int32, (1, wide), 1) < HEAD

    def pairs_of(a, j):
        return a[j * wide : (j + 1) * wide, :]

    def twice(a):
        return jnp.concatenate([a[pairs * wide :, :]] * 2, axis=0)

    def pack(values, keys):
        out = []
        for j in range(pairs):
            full = nt(pairs_of(values, j), pairs_of(keys, j))
            out.append(jnp.where(lane_low, full[:HEAD, :], full[HEAD:, :]))
        if odd:
            full = nt(values[pairs * wide :, :], twice(keys))
            out.append(jnp.where(lane_low, full[: HEAD // 2, :], full[HEAD // 2 :, :]))
        return jnp.concatenate(out, axis=0)

    def opened(state):
        out = []
        for j in range(pairs + odd):
            size = HEAD if j < pairs else HEAD // 2
            rows_of = state[j * HEAD : j * HEAD + size, :]
            out.append(
                jnp.concatenate(
                    [jnp.where(lane_low, rows_of, 0.0), jnp.where(lane_low, 0.0, rows_of)], axis=0
                ).astype(bf16)
            )
        return out

    def from_keys(blocks, a):
        out = [nn(blocks[j], pairs_of(a, j)) for j in range(pairs)]
        if odd:
            out.append(nn(blocks[pairs], twice(a)))
        return jnp.concatenate(out, axis=0)

    def from_values(blocks, a):
        out = [tn(blocks[j], pairs_of(a, j)) for j in range(pairs)]
        if odd:
            full = tn(blocks[pairs], a[pairs * wide :, :])
            out.append(full[:HEAD, :] + full[HEAD:, :])
        return jnp.concatenate(out, axis=0)

    def scaled(logs, state):
        out = []
        for j in range(pairs + odd):
            size = HEAD if j < pairs else HEAD // 2
            out.append(jnp.exp(logs[j]) * state[j * HEAD : j * HEAD + size, :])
        return jnp.concatenate(out, axis=0)

    row_at = lax.broadcasted_iota(jnp.int32, (LOGROWS, wide), 0)

    def log_rows(logs):
        rows_f = jnp.zeros((LOGROWS, wide), f32)
        for j, log in enumerate(logs):
            high, low = split(log)
            rows_f = jnp.where(row_at == 2 * j, high.astype(f32), rows_f)
            rows_f = jnp.where(row_at == 2 * j + 1, low.astype(f32), rows_f)
        return rows_f.astype(bf16)

    def read(ref, at):
        state = ref[at, 0:packed, :].astype(f32)
        tail = ref[at, packed : packed + LOGROWS, :].astype(f32)
        logs = [tail[2 * j : 2 * j + 1, :] + tail[2 * j + 1 : 2 * j + 2, :] for j in range(pairs + odd)]
        return state, logs

    def added(a, b):
        return [p + q for p, q in zip(a, b)]

    s_at = lax.broadcasted_iota(jnp.int32, (tokens, tokens), 0)
    t_at = lax.broadcasted_iota(jnp.int32, (tokens, tokens), 1)
    upper, lower = s_at <= t_at, s_at >= t_at
    upper_b, lower_b = upper.astype(f32).astype(bf16), lower.astype(f32).astype(bf16)
    ones = jnp.ones((LOGROWS, tokens), bf16)
    lb = jnp.broadcast_to(lb_ref[...], (tokens, width)).T
    f_in = f_ref[...].astype(f32)
    f_sig = jax.nn.sigmoid(f_in)
    key = (1.0 - lb) * jax.nn.sigmoid(-f_in)
    high, low = split(jnp.log1p(-key))
    cumulative = nn(high, upper_b) + nn(low, upper_b)
    growth = jnp.exp(cumulative)
    q_in = q_ref[...].astype(f32)
    q_sig = jax.nn.sigmoid(q_in)
    query = q_in * q_sig
    q_dec = (query * growth).astype(bf16)
    g = g_ref[...]
    logs = []
    for j in range(pairs):
        logs.append((nt(ones, pairs_of(high, j)) + nt(ones, pairs_of(low, j)))[0:1, :])
    if odd:
        logs.append((nt(ones, twice(high)) + nt(ones, twice(low)))[0:1, :])
    tail = log_rows(logs)
    b1[here, 0:packed, :] = pack(g, q_dec).astype(bf16)
    b1[here, packed : packed + LOGROWS, :] = tail
    pl.semaphore_wait(barrier, inner + outer + n_tp - 3)
    for k in range(1, inner):
        copy_b1(k, here).start()
    for k in range(1, n_tp):
        copy_w(k).start()

    value = nt(w_ref[...], x_ref[...]).astype(bf16)
    closing = cumulative[:, tokens - 1 : tokens]
    k_end = (key * jnp.exp(closing - cumulative)).astype(bf16)
    update = pack(value, k_end)
    f1[here, 0:packed, :] = update.astype(bf16)
    f1[here, packed : packed + LOGROWS, :] = tail
    for k in range(1, inner):
        copy_f1(k, here).start()
    shrinking = jnp.exp(-cumulative)
    k_dec = (key * shrinking).astype(bf16)

    def of(a, h):
        return a[h * HEAD : (h + 1) * HEAD, :]

    mixing = [jnp.where(upper, tn(of(k_dec, h), of(q_dec, h)), 0.0).astype(bf16) for h in range(heads)]
    gv_local = jnp.concatenate([nt(of(g, h), mixing[h]) for h in range(heads)], axis=0)
    gvk[here, 0] = gv_local.astype(bf16)
    gvk[here, 1] = k_end
    for k in range(1, inner):
        copy_k(k, here).start()
    xt[...] = x_ref[...].T.reshape(xt.shape)
    for k in range(1, inner):
        copy_x(k).start()
    xg[:, lead, :, own_lanes] = xt[:, here, lead]

    for k in range(1, inner):
        copy_b1(k, source(k)).wait_recv()
    inside, after = [None] * inner, [None] * inner
    running = jnp.zeros((packed, wide), f32)
    plane_logs = [jnp.zeros((1, wide), f32) for _ in range(pairs + odd)]
    for j in reversed(range(inner)):
        inside[j], after[j] = running, plane_logs
        state, own_logs = read(b1, j)
        running = state + scaled(own_logs, running)
        plane_logs = added(plane_logs, own_logs)
    plane_tail = log_rows(plane_logs)
    bmsg[0:packed, :] = running.astype(bf16)
    bmsg[packed : packed + LOGROWS, :] = plane_tail

    def each(lo, hi, act):
        def step(i, carried):
            act(i)
            return carried

        lax.fori_loop(lo, hi, step, 0)

    each(outer - plane, outer, lambda k: copy_b2(k, plane).start())

    for k in range(1, inner):
        copy_f1(k, source(k)).wait_recv()
    running = jnp.zeros((packed, wide), f32)
    before = [jnp.zeros((1, wide), f32) for _ in range(pairs + odd)]
    incoming = running
    in_logs = before
    for j in range(inner):
        incoming = jnp.where(here == j, running, incoming)
        in_logs = [jnp.where(here == j, p, q) for p, q in zip(before, in_logs)]
        state, own_logs = read(f1, j)
        running = state + scaled(own_logs, running)
        before = added(before, own_logs)
    fmsg[0:packed, :] = running.astype(bf16)
    fmsg[packed : packed + LOGROWS, :] = plane_tail
    each(1, outer - plane, lambda k: copy_f2(k, plane).start())

    pairing = [jnp.where(upper, tn(of(value, h), of(g, h)), 0.0).astype(bf16) for h in range(heads)]
    gk_local = jnp.concatenate([nt(of(q_dec, h), pairing[h]) for h in range(heads)], axis=0)
    gq_local = jnp.concatenate([nn(of(k_dec, h), pairing[h]) for h in range(heads)], axis=0)

    for k in range(1, inner):
        lanes = pl.ds(pl.multiple_of(source(k) * tokens, tokens), tokens)
        rc(xt.at[:, 0, lead], xg.at[:, lead, :, lanes], x_send, x_recv, k, near(k)).wait_recv()
    if part > 1:
        copy_r(lead).start()

    empty = jnp.zeros((packed, wide), f32)
    none = [jnp.zeros((1, wide), f32) for _ in range(pairs + odd)]

    def entering(ref, copy, count, place, distance):
        def step(i, carried):
            total, weight = carried
            copy(distance(i), place(i)).wait_recv()
            state, own_logs = read(ref, place(i))
            return total + scaled(weight, state), added(weight, own_logs)

        return lax.fori_loop(0, count, step, (empty, none))[0]

    below = entering(
        b2, copy_b2, outer - 1 - plane, lambda i: plane + 1 + i, lambda i: outer - 1 - i
    )
    outgoing = empty
    for k in range(1, inner):
        copy_k(k, source(k)).wait_recv()
    for j in range(inner):
        grad_state = inside[j] + scaled(after[j], below)
        outgoing = jnp.where(here == j, grad_state, outgoing)
        value_grad = gvk[j, 0].astype(f32) + from_keys(opened(grad_state), gvk[j, 1])
        dvp[:, j * tokens : (j + 1) * tokens] = value_grad.astype(bf16)
    for k in range(1, n_tp):
        copy_m(k).start()
    if part > 1:
        copy_r(1 - lead).wait_recv()
    for z in range(outer):
        pieces = [nt(dvp[...], xg[z, p]) for p in range(part)]
        pmsg[z] = jnp.concatenate(pieces, axis=1).astype(bf16)
    for k in range(1, outer):
        copy_p(k).start()

    def rows_half(a, slot):
        dvs[slot] = a.T
        return dvs[slot, pl.ds(pl.multiple_of(core * half, half), half), :]

    gx = nn(rows_half(dvp[:, own_lanes], 0), w_ref[...]).astype(bf16).astype(f32)
    for k in range(1, n_tp):
        copy_w(k).wait_recv()
        copy_m(k).wait_recv()
        gx = gx + nn(rows_half(dvm[k - 1], k), w_all[k - 1]).astype(bf16).astype(f32)
    gx_ref[...] = gx.astype(bf16)

    above = entering(f2, copy_f2, plane, lambda i: plane - 1 - i, lambda i: i + 1)
    incoming = incoming + scaled(in_logs, above)
    grad_query = growth * (gq_local + from_values(opened(incoming), g))
    remaining = jnp.exp(closing - cumulative)
    grad_key = shrinking * gk_local + remaining * from_values(opened(outgoing), value)
    product = outgoing * (scaled(logs, incoming) + update)
    p_high, p_low = split(product)
    bound = []
    for j in range(pairs + odd):
        size = HEAD if j < pairs else HEAD // 2
        every = jnp.ones((size, tokens), bf16)
        at = slice(j * HEAD, j * HEAD + size)
        full = tn(p_high[at, :], every) + tn(p_low[at, :], every)
        bound.append(full if j < pairs else full[:HEAD, :] + full[HEAD:, :])
    boundary = jnp.concatenate(bound, axis=0)
    c_high, c_low = split(query * grad_query - key * grad_key)
    grad_decay = nn(c_high, lower_b) + nn(c_low, lower_b) + boundary
    gq_ref[...] = (grad_query * (q_sig * (1.0 + q_in * (1.0 - q_sig)))).astype(bf16)
    gf_ref[...] = (-(grad_key - grad_decay / (1.0 - key)) * key * f_sig).astype(bf16)

    total = pmsg[plane].astype(f32)
    for k in range(1, outer):
        copy_p(k).wait_recv()
        total = total + pin[k - 1].astype(f32)
    gw_ref[...] = total

    for k in range(1, n_tp):
        copy_w(k).wait_send()
        copy_m(k).wait_send()
    if part > 1:
        copy_r(lead).wait_send()
    for k in range(1, inner):
        copy_b1(k, here).wait_send()
        copy_f1(k, here).wait_send()
        copy_k(k, here).wait_send()
        copy_x(k).wait_send()
    each(outer - plane, outer, lambda k: copy_b2(k, plane).wait_send())
    each(1, outer - plane, lambda k: copy_f2(k, plane).wait_send())
    for k in range(1, outer):
        copy_p(k).wait_send()


def on_device(n, n_tp, block_input, value_weight, query_pre, forget_pre, lower_bound, out_grad):
    tokens, depth = block_input.shape
    width = query_pre.shape[1]
    heads = width // HEAD
    rows = depth // n
    inner = 1
    while n % (inner * 2) == 0 and (inner * 2) ** 2 <= n:
        inner *= 2
    outer = n // inner
    part = 2 if n_tp == 2 and rows % 32 == 0 else 1
    message = (heads // 2) * HEAD + (heads % 2) * HEAD // 2 + LOGROWS
    dma = pltpu.SemaphoreType.DMA
    vmem = pl.BlockSpec(memory_space=pltpu.VMEM)
    gq, gf, gx, gw = pl.pallas_call(
        functools.partial(kernel, inner, outer, n_tp, part),
        out_shape=(
            jax.ShapeDtypeStruct((width, tokens), bf16),
            jax.ShapeDtypeStruct((width, tokens), bf16),
            jax.ShapeDtypeStruct((tokens // n_tp, depth), bf16),
            jax.ShapeDtypeStruct((width, rows), f32),
        ),
        in_specs=[vmem] * 6,
        out_specs=(vmem,) * 4,
        scratch_shapes=[
            pltpu.VMEM((n_tp - 1, width, depth), bf16),
            pltpu.VMEM((outer, inner, part, rows // part, tokens), bf16),
            pltpu.VMEM((outer, part, rows // part, inner * tokens), bf16),
            pltpu.VMEM((inner, message, 2 * HEAD), bf16),
            pltpu.VMEM((inner, message, 2 * HEAD), bf16),
            pltpu.VMEM((message, 2 * HEAD), bf16),
            pltpu.VMEM((message, 2 * HEAD), bf16),
            pltpu.VMEM((outer, message, 2 * HEAD), bf16),
            pltpu.VMEM((outer, message, 2 * HEAD), bf16),
            pltpu.VMEM((inner, 2, width, tokens), bf16),
            pltpu.VMEM((width, inner * tokens), bf16),
            pltpu.VMEM((n_tp - 1, width, tokens), bf16),
            pltpu.VMEM((outer, width, rows), bf16),
            pltpu.VMEM((outer - 1, width, rows), bf16),
            pltpu.VMEM((n_tp, tokens, width), bf16),
            dma((n_tp - 1,)), dma((n_tp - 1,)),
            dma((inner - 1,)), dma((inner - 1,)),
            dma((1,)), dma((1,)),
            dma((inner - 1,)), dma((inner - 1,)),
            dma((inner - 1,)), dma((inner - 1,)),
            dma((outer - 1,)), dma((outer - 1,)),
            dma((outer - 1,)), dma((outer - 1,)),
            dma((inner - 1,)), dma((inner - 1,)),
            dma((n_tp - 1,)), dma((n_tp - 1,)),
            dma((outer - 1,)), dma((outer - 1,)),
        ],
        compiler_params=pltpu.CompilerParams(
            collective_id=0, has_side_effects=True, vmem_limit_bytes=60 * 1024 * 1024
        ),
    )(block_input, value_weight.T, query_pre.T, forget_pre.T, lower_bound[None, :], out_grad.T)
    return gq.T, gf.T, gx, gw.T


def solution(mesh):
    n, n_tp = mesh.shape["sp"], mesh.shape["tp"]
    in_specs = (P("sp", None), P(None, "tp"), P("sp", "tp"), P("sp", "tp"), P("tp"), P("sp", "tp"))
    out_specs = (P("sp", "tp"), P("sp", "tp"), P(("sp", "tp"), None), P("sp", "tp"))
    return jax.shard_map(
        functools.partial(on_device, n, n_tp),
        mesh=mesh, in_specs=in_specs, out_specs=out_specs, check_vma=False,
    )
```

time: 65.1 us -> 30.7 us (0.47)
  the two profiles are of different devices: /device:TPU:30 before, /device:TPU:0 now
where the time goes in v2:
time: 30.7 us; the launch traced here: 30.2 us
  Pallas kernels  25.1 us (82%)
  local copies, waits for them, and re-layouts  4.41 us (14%)
  between operations  0.65 us (2%)
    pallas_call x1, Pallas kernels, on_device(): pl.pallas_call(functools.partial(kernel, inner, outer, n_tp, part), out_s...  25.1 us
    unnamed x8, local copies, waits for them, and re-layouts  4.41 us

profile of v2, /device:TPU:0, one launch (start us, length us, event | category | flops | bytes accessed | tf_op | source)
XLA Modules:
  0.0 30.2 jit_solution(16747269319451081716)
XLA Ops:
  0.6 25.1 %shard_map.93 = (bf16[192,128]{1,0:T(8,128)(2,1)}, bf16[192,128]{1,0:T(8,128)(2,1)}, bf16[64,2048]{1,0:T(8,128)(2,1)}, f32[192,128]{1,0:T(8,128)}) custom-call(bf16[128,2048]{1,0:T(8,128)(2,1)} %x_ref.1, bf16[192,2048]{1,0:T(8,128)(2,1)} %bitcast.8, bf16[192,128]{1,0:T(8,128)(2,1)} %bitcast.10, bf16[192,128]{1,0:T(8,128)(2,1)} %bitcast.11, ...), custom_call_target="tpu_custom_call" | custom-call | tf_op jit(solution)/shard_map/pallas_call | solution.py:380
  25.8 0.0 copy-start.1
  25.8 1.4 %copy.14 = bf16[128,192]{0,1:T(8,128)(2,1)} copy(bf16[128,192]{0,1:T(8,128)(2,1)} %bitcast.14) | data formatting | bytes 98304
  27.2 0.0 copy-done.1
  27.2 0.6 %copy.15 = bf16[128,192]{0,1:T(8,128)(2,1)} copy(bf16[128,192]{0,1:T(8,128)(2,1)S(1)} %bitcast.13) | data formatting | bytes 98304
  27.8 0.0 copy-start
  27.8 1.7 %copy.16 = bf16[64,2048]{1,0:T(8,128)(2,1)} copy(bf16[64,2048]{1,0:T(8,128)(2,1)} %get-tuple-element.18) | data formatting | bytes 524288
  29.5 0.0 copy-done
  29.5 0.6 %copy.17 = f32[128,192]{0,1:T(8,128)} copy(f32[128,192]{0,1:T(8,128)S(1)} %bitcast.9) | data formatting | bytes 196608
Async XLA Ops:
  25.8 1.4 %copy-start.1 = (bf16[192,128]{1,0:T(8,128)(2,1)S(1)}, bf16[192,128]{1,0:T(8,128)(2,1)}, u32[]{:S(2)}) copy-start(bf16[192,128]{1,0:T(8,128)(2,1)} %get-tuple-element.9) | copy-start | bytes 147460
  27.8 1.7 %copy-start = (f32[192,128]{1,0:T(8,128)S(1)}, f32[192,128]{1,0:T(8,128)}, u32[]{:S(2)}) copy-start(f32[192,128]{1,0:T(8,128)} %get-tuple-element.11) | copy-start | bytes 294916

commit v3 on v2

--- a/solution.py
+++ b/solution.py
@@ -32,8 +32,9 @@
 
 def kernel(
     inner, outer, n_tp, part,
-    x_ref, w_ref, q_ref, f_ref, lb_ref, g_ref,
+    x_in, w_in, q_hbm, f_hbm, lb_ref, g_in,
     gq_ref, gf_ref, gx_ref, gw_ref,
+    x_ref, w_ref, q_ref, f_ref, g_ref, in_sem,
     w_all, xt, xg, b1, f1, bmsg, fmsg, b2, f2, gvk, dvp, dvm, pmsg, pin, dvs,
     w_send, w_recv, x_send, x_recv, r_send, r_recv, b1_send, b1_recv, f1_send, f1_recv,
     b2_send, b2_recv, f2_send, f2_recv, k_send, k_recv, m_send, m_recv, p_send, p_recv,
@@ -60,6 +61,14 @@
     def rc(src, dst, send, recv, k, to):
         return pltpu.make_async_remote_copy(src, dst, send.at[k - 1], recv.at[k - 1], to, MESH)
 
+    loads = [
+        pltpu.make_async_copy(src, dst, in_sem.at[i])
+        for i, (src, dst) in enumerate(
+            ((f_hbm, f_ref), (q_hbm, q_ref), (g_in, g_ref), (w_in, w_ref), (x_in, x_ref))
+        )
+    ]
+    for load in loads:
+        load.start()
     barrier = pltpu.get_barrier_semaphore()
     for to, count in ((near, inner), (column, outer), (mate, n_tp)):
         for k in range(1, count):
@@ -86,8 +95,9 @@
     def copy_f1(k, at):
         return rc(f1.at[at], f1.at[at], f1_send, f1_recv, k, near(k))
 
-    def copy_k(k, at):
-        return rc(gvk.at[at], gvk.at[at], k_send, k_recv, k, near(k))
+    def copy_k(k, at, h):
+        each_h = (inner - 1) * h + k
+        return rc(gvk.at[at, h], gvk.at[at, h], k_send, k_recv, each_h, near(k))
 
     def copy_b2(k, at):
         return rc(bmsg, b2.at[at], b2_send, b2_recv, k, column(k))
@@ -98,8 +108,11 @@
     def copy_m(k):
         return rc(dvp.at[:, own_lanes], dvm.at[k - 1], m_send, m_recv, k, mate(k))
 
-    def copy_p(k):
-        return rc(pmsg.at[lax.rem(plane + k, outer)], pin.at[k - 1], p_send, p_recv, k, column(k))
+    def copy_p(k, h):
+        return rc(
+            pmsg.at[h, lax.rem(plane + k, outer)], pin.at[k - 1, h],
+            p_send, p_recv, (outer - 1) * h + k, column(k),
+        )
 
     def source(k):
         return lax.rem(here + inner - k, inner)
@@ -134,12 +147,6 @@
             )
         return out
 
-    def from_keys(blocks, a):
-        out = [nn(blocks[j], pairs_of(a, j)) for j in range(pairs)]
-        if odd:
-            out.append(nn(blocks[pairs], twice(a)))
-        return jnp.concatenate(out, axis=0)
-
     def from_values(blocks, a):
         out = [tn(blocks[j], pairs_of(a, j)) for j in range(pairs)]
         if odd:
@@ -179,16 +186,19 @@
     upper_b, lower_b = upper.astype(f32).astype(bf16), lower.astype(f32).astype(bf16)
     ones = jnp.ones((LOGROWS, tokens), bf16)
     lb = jnp.broadcast_to(lb_ref[...], (tokens, width)).T
+    loads[0].wait()
     f_in = f_ref[...].astype(f32)
     f_sig = jax.nn.sigmoid(f_in)
     key = (1.0 - lb) * jax.nn.sigmoid(-f_in)
     high, low = split(jnp.log1p(-key))
     cumulative = nn(high, upper_b) + nn(low, upper_b)
     growth = jnp.exp(cumulative)
+    loads[1].wait()
     q_in = q_ref[...].astype(f32)
     q_sig = jax.nn.sigmoid(q_in)
     query = q_in * q_sig
     q_dec = (query * growth).astype(bf16)
+    loads[2].wait()
     g = g_ref[...]
     logs = []
     for j in range(pairs):
@@ -201,8 +211,10 @@
     pl.semaphore_wait(barrier, inner + outer + n_tp - 3)
     for k in range(1, inner):
         copy_b1(k, here).start()
+    loads[3].wait()
     for k in range(1, n_tp):
         copy_w(k).start()
+    loads[4].wait()
 
     value = nt(w_ref[...], x_ref[...]).astype(bf16)
     closing = cumulative[:, tokens - 1 : tokens]
@@ -218,16 +230,16 @@
     def of(a, h):
         return a[h * HEAD : (h + 1) * HEAD, :]
 
-    mixing = [jnp.where(upper, tn(of(k_dec, h), of(q_dec, h)), 0.0).astype(bf16) for h in range(heads)]
-    gv_local = jnp.concatenate([nt(of(g, h), mixing[h]) for h in range(heads)], axis=0)
-    gvk[here, 0] = gv_local.astype(bf16)
-    gvk[here, 1] = k_end
-    for k in range(1, inner):
-        copy_k(k, here).start()
     xt[...] = x_ref[...].T.reshape(xt.shape)
     for k in range(1, inner):
         copy_x(k).start()
     xg[:, lead, :, own_lanes] = xt[:, here, lead]
+    for h in range(heads):
+        mixing = jnp.where(upper, tn(of(k_dec, h), of(q_dec, h)), 0.0).astype(bf16)
+        gvk[here, h, 0] = nt(of(g, h), mixing).astype(bf16)
+        gvk[here, h, 1] = of(k_end, h)
+        for k in range(1, inner):
+            copy_k(k, here, h).start()
 
     for k in range(1, inner):
         copy_b1(k, source(k)).wait_recv()
@@ -294,22 +306,29 @@
         b2, copy_b2, outer - 1 - plane, lambda i: plane + 1 + i, lambda i: outer - 1 - i
     )
     outgoing = empty
-    for k in range(1, inner):
-        copy_k(k, source(k)).wait_recv()
+    opens = []
     for j in range(inner):
         grad_state = inside[j] + scaled(after[j], below)
         outgoing = jnp.where(here == j, grad_state, outgoing)
-        value_grad = gvk[j, 0].astype(f32) + from_keys(opened(grad_state), gvk[j, 1])
-        dvp[:, j * tokens : (j + 1) * tokens] = value_grad.astype(bf16)
+        opens.append(opened(grad_state))
+    if part > 1:
+        copy_r(1 - lead).wait_recv()
+    for h in range(heads):
+        for k in range(1, inner):
+            copy_k(k, source(k), h).wait_recv()
+        at = slice(h * HEAD, (h + 1) * HEAD)
+        for j in range(inner):
+            block = opens[j][h // 2][h % 2 * HEAD : (h % 2 + 1) * HEAD, :]
+            doubled = jnp.concatenate([gvk[j, h, 1]] * 2, axis=0)
+            value_grad = gvk[j, h, 0].astype(f32) + nn(block, doubled)
+            dvp[at, j * tokens : (j + 1) * tokens] = value_grad.astype(bf16)
+        for z in range(outer):
+            pieces = [nt(dvp[at, :], xg[z, p]) for p in range(part)]
+            pmsg[h, z] = jnp.concatenate(pieces, axis=1).astype(bf16)
+        for k in reversed(range(1, outer)):
+            copy_p(k, h).start()
     for k in range(1, n_tp):
         copy_m(k).start()
-    if part > 1:
-        copy_r(1 - lead).wait_recv()
-    for z in range(outer):
-        pieces = [nt(dvp[...], xg[z, p]) for p in range(part)]
-        pmsg[z] = jnp.concatenate(pieces, axis=1).astype(bf16)
-    for k in range(1, outer):
-        copy_p(k).start()
 
     def rows_half(a, slot):
         dvs[slot] = a.T
@@ -342,11 +361,12 @@
     gq_ref[...] = (grad_query * (q_sig * (1.0 + q_in * (1.0 - q_sig)))).astype(bf16)
     gf_ref[...] = (-(grad_key - grad_decay / (1.0 - key)) * key * f_sig).astype(bf16)
 
-    total = pmsg[plane].astype(f32)
-    for k in range(1, outer):
-        copy_p(k).wait_recv()
-        total = total + pin[k - 1].astype(f32)
-    gw_ref[...] = total
+    for h in range(heads):
+        total = pmsg[h, plane].astype(f32)
+        for k in range(1, outer):
+            copy_p(k, h).wait_recv()
+            total = total + pin[k - 1, h].astype(f32)
+        gw_ref[h * HEAD : (h + 1) * HEAD, :] = total
 
     for k in range(1, n_tp):
         copy_w(k).wait_send()
@@ -356,12 +376,19 @@
     for k in range(1, inner):
         copy_b1(k, here).wait_send()
         copy_f1(k, here).wait_send()
-        copy_k(k, here).wait_send()
+        for h in range(heads):
+            copy_k(k, here, h).wait_send()
         copy_x(k).wait_send()
     each(outer - plane, outer, lambda k: copy_b2(k, plane).wait_send())
     each(1, outer - plane, lambda k: copy_f2(k, plane).wait_send())
     for k in range(1, outer):
-        copy_p(k).wait_send()
+        for h in range(heads):
+            copy_p(k, h).wait_send()
+
+
+def hand_on(*refs):
+    for source, target in zip(refs[:4], refs[4:]):
+        target[...] = source[...]
 
 
 def on_device(n, n_tp, block_input, value_weight, query_pre, forget_pre, lower_bound, out_grad):
@@ -377,7 +404,8 @@
     message = (heads // 2) * HEAD + (heads % 2) * HEAD // 2 + LOGROWS
     dma = pltpu.SemaphoreType.DMA
     vmem = pl.BlockSpec(memory_space=pltpu.VMEM)
-    gq, gf, gx, gw = pl.pallas_call(
+    anywhere = pl.BlockSpec(memory_space=pl.ANY)
+    results = pl.pallas_call(
         functools.partial(kernel, inner, outer, n_tp, part),
         out_shape=(
             jax.ShapeDtypeStruct((width, tokens), bf16),
@@ -385,9 +413,15 @@
             jax.ShapeDtypeStruct((tokens // n_tp, depth), bf16),
             jax.ShapeDtypeStruct((width, rows), f32),
         ),
-        in_specs=[vmem] * 6,
+        in_specs=[anywhere] * 4 + [vmem, anywhere],
         out_specs=(vmem,) * 4,
         scratch_shapes=[
+            pltpu.VMEM((tokens, depth), bf16),
+            pltpu.VMEM((width, depth), bf16),
+            pltpu.VMEM((width, tokens), bf16),
+            pltpu.VMEM((width, tokens), bf16),
+            pltpu.VMEM((width, tokens), bf16),
+            dma((5,)),
             pltpu.VMEM((n_tp - 1, width, depth), bf16),
             pltpu.VMEM((outer, inner, part, rows // part, tokens), bf16),
             pltpu.VMEM((outer, part, rows // part, inner * tokens), bf16),
@@ -397,11 +431,11 @@
             pltpu.VMEM((message, 2 * HEAD), bf16),
             pltpu.VMEM((outer, message, 2 * HEAD), bf16),
             pltpu.VMEM((outer, message, 2 * HEAD), bf16),
-            pltpu.VMEM((inner, 2, width, tokens), bf16),
+            pltpu.VMEM((inner, heads, 2, HEAD, tokens), bf16),
             pltpu.VMEM((width, inner * tokens), bf16),
             pltpu.VMEM((n_tp - 1, width, tokens), bf16),
-            pltpu.VMEM((outer, width, rows), bf16),
-            pltpu.VMEM((outer - 1, width, rows), bf16),
+            pltpu.VMEM((heads, outer, HEAD, rows), bf16),
+            pltpu.VMEM((outer - 1, heads, HEAD, rows), bf16),
             pltpu.VMEM((n_tp, tokens, width), bf16),
             dma((n_tp - 1,)), dma((n_tp - 1,)),
             dma((inner - 1,)), dma((inner - 1,)),
@@ -410,14 +444,20 @@
             dma((inner - 1,)), dma((inner - 1,)),
             dma((outer - 1,)), dma((outer - 1,)),
             dma((outer - 1,)), dma((outer - 1,)),
-            dma((inner - 1,)), dma((inner - 1,)),
+            dma((heads * (inner - 1),)), dma((heads * (inner - 1),)),
             dma((n_tp - 1,)), dma((n_tp - 1,)),
-            dma((outer - 1,)), dma((outer - 1,)),
+            dma((heads * (outer - 1),)), dma((heads * (outer - 1),)),
         ],
         compiler_params=pltpu.CompilerParams(
             collective_id=0, has_side_effects=True, vmem_limit_bytes=60 * 1024 * 1024
         ),
     )(block_input, value_weight.T, query_pre.T, forget_pre.T, lower_bound[None, :], out_grad.T)
+    gq, gf, gx, gw = pl.pallas_call(
+        hand_on,
+        out_shape=tuple(jax.ShapeDtypeStruct(a.shape, a.dtype) for a in results),
+        in_specs=[vmem] * 4,
+        out_specs=(vmem,) * 4,
+    )(*results)
     return gq.T, gf.T, gx, gw.T
 
 

time: 30.7 us -> 26.3 us (0.86); the launches traced: 30.2 us -> 26.1 us
  local copies, waits for them, and re-layouts: 4.41 us -> 0 us
  Pallas kernels: 25.1 us -> 25.5 us
    unnamed x8 -> x0, local copies, waits for them, and re-layouts: 4.41 us -> none
    pallas_call x0 -> x1, Pallas kernels: none -> 1.8 us  [on_device(): pl.pallas_call(hand_on, out_shape=tuple((jax.ShapeDtypeStruct(a.shape, a....]
    pallas_call x1, Pallas kernels: 25.1 us -> 23.7 us  [on_device(): pl.pallas_call(functools.partial(kernel, inner, outer, n_tp, part), out_s...]
where the time goes in v3:
time: 26.3 us; the launch traced here: 26.1 us
  Pallas kernels  25.5 us (97%)
  between operations  0.64 us (2%)
    pallas_call x1, Pallas kernels, on_device(): pl.pallas_call(functools.partial(kernel, inner, outer, n_tp, part), out_s...  23.7 us
    pallas_call x1, Pallas kernels, on_device(): pl.pallas_call(hand_on, out_shape=tuple((jax.ShapeDtypeStruct(a.shape, a....  1.8 us

profile of v3, /device:TPU:0, one launch (start us, length us, event | category | flops | bytes accessed | tf_op | source)
XLA Modules:
  0.0 26.1 jit_solution(8934235124968859199)
XLA Ops:
  0.6 23.7 %shard_map.93 = (bf16[192,128]{1,0:T(8,128)(2,1)}, bf16[192,128]{1,0:T(8,128)(2,1)}, bf16[64,2048]{1,0:T(8,128)(2,1)}, f32[192,128]{1,0:T(8,128)}) custom-call(bf16[128,2048]{1,0:T(8,128)(2,1)} %x_in.1, bf16[192,2048]{1,0:T(8,128)(2,1)} %bitcast.8, bf16[192,128]{1,0:T(8,128)(2,1)} %bitcast.9, bf16[192,128]{1,0:T(8,128)(2,1)} %bitcast.10, f32[1,192]{1,0:T(1,128)} %bitcast.12, ...), custom_call_target="tpu_custom_call" | custom-call | tf_op jit(solution)/shard_map/pallas_call | solution.py:408
  24.3 1.8 %shard_map.94 = (bf16[192,128]{1,0:T(8,128)(2,1)}, bf16[192,128]{1,0:T(8,128)(2,1)}, bf16[64,2048]{1,0:T(8,128)(2,1)}, f32[192,128]{1,0:T(8,128)}) custom-call(bf16[192,128]{1,0:T(8,128)(2,1)} %get-tuple-element.12.refs_0_, bf16[192,128]{1,0:T(8,128)(2,1)} %get-tuple-element.13.refs_1_, bf16[64,2048]{1,0:T(8,128)(2,1)} %get-tuple-element.14.refs_2_, ...), custom_call_target="tpu_custom_call" | custom-call | tf_op jit(solution)/shard_map/pallas_call | solution.py:455

commit v4 on v3

--- a/solution.py
+++ b/solution.py
@@ -387,8 +387,13 @@
 
 
 def hand_on(*refs):
-    for source, target in zip(refs[:4], refs[4:]):
-        target[...] = source[...]
+    copies = [
+        pltpu.make_async_copy(refs[i], refs[4 + i], refs[8].at[i]) for i in range(4)
+    ]
+    for copy in copies:
+        copy.start()
+    for copy in copies:
+        copy.wait()
 
 
 def on_device(n, n_tp, block_input, value_weight, query_pre, forget_pre, lower_bound, out_grad):
@@ -408,10 +413,10 @@
     results = pl.pallas_call(
         functools.partial(kernel, inner, outer, n_tp, part),
         out_shape=(
-            jax.ShapeDtypeStruct((width, tokens), bf16),
-            jax.ShapeDtypeStruct((width, tokens), bf16),
-            jax.ShapeDtypeStruct((tokens // n_tp, depth), bf16),
-            jax.ShapeDtypeStruct((width, rows), f32),
+            pltpu.VMEM((width, tokens), bf16),
+            pltpu.VMEM((width, tokens), bf16),
+            pltpu.VMEM((tokens // n_tp, depth), bf16),
+            pltpu.VMEM((width, rows), f32),
         ),
         in_specs=[anywhere] * 4 + [vmem, anywhere],
         out_specs=(vmem,) * 4,
@@ -456,8 +461,9 @@
         hand_on,
         out_shape=tuple(jax.ShapeDtypeStruct(a.shape, a.dtype) for a in results),
         in_specs=[vmem] * 4,
-        out_specs=(vmem,) * 4,
-    )(*results)
+        out_specs=(anywhere,) * 4,
+        scratch_shapes=[dma((4,))],
+    )(*[pltpu.with_memory_space_constraint(a, pltpu.VMEM) for a in results])
     return gq.T, gf.T, gx, gw.T
 
 

time: 26.3 us -> 24.5 us (0.932)
  Pallas kernels: 25.5 us -> 23.7 us
    pallas_call x1, Pallas kernels: 1.8 us -> 0.8 us  [on_device(): pl.pallas_call(hand_on, out_shape=tuple((jax.ShapeDtypeStruct(a.shape, a....]
    pallas_call x1, Pallas kernels: 23.7 us -> 22.9 us  [on_device(): pl.pallas_call(functools.partial(kernel, inner, outer, n_tp, part), out_s...]
where the time goes in v4:
time: 24.5 us; the launch traced here: 24.3 us
  Pallas kernels  23.7 us (97%)
  between operations  0.64 us (3%)
    pallas_call x1, Pallas kernels, on_device(): pl.pallas_call(functools.partial(kernel, inner, outer, n_tp, part), out_s...  22.9 us
    pallas_call x1, Pallas kernels, on_device(): pl.pallas_call(hand_on, out_shape=tuple((jax.ShapeDtypeStruct(a.shape, a....  0.8 us

profile of v4, /device:TPU:0, one launch (start us, length us, event | category | flops | bytes accessed | tf_op | source)
XLA Modules:
  0.0 24.3 jit_solution(1159317426013871833)
XLA Ops:
  0.6 22.9 %shard_map.93 = (bf16[192,128]{1,0:T(8,128)(2,1)S(1)}, bf16[192,128]{1,0:T(8,128)(2,1)S(1)}, bf16[64,2048]{1,0:T(8,128)(2,1)S(1)}, f32[192,128]{1,0:T(8,128)S(1)}) custom-call(bf16[128,2048]{1,0:T(8,128)(2,1)} %x_in.1, bf16[192,2048]{1,0:T(8,128)(2,1)} %bitcast.8, bf16[192,128]{1,0:T(8,128)(2,1)} %bitcast.9, bf16[192,128]{1,0:T(8,128)(2,1)} %bitcast.10, ...), custom_call_target="tpu_custom_call" | custom-call | tf_op jit(solution)/shard_map/pallas_call | solution.py:413
  23.5 0.8 %shard_map.94 = (bf16[192,128]{1,0:T(8,128)(2,1)}, bf16[192,128]{1,0:T(8,128)(2,1)}, bf16[64,2048]{1,0:T(8,128)(2,1)}, f32[192,128]{1,0:T(8,128)}) custom-call(bf16[192,128]{1,0:T(8,128)(2,1)S(1)} %get-tuple-element.12.refs_0_, bf16[192,128]{1,0:T(8,128)(2,1)S(1)} %get-tuple-element.13.refs_1_, bf16[64,2048]{1,0:T(8,128)(2,1)S(1)} %get-tuple-element.14.refs_2_, ...), custom_call_target="tpu_custom_call" | custom-call | tf_op jit(solution)/shard_map/pallas_call | solution.py:460

commit v5 on v4

--- a/solution.py
+++ b/solution.py
@@ -215,6 +215,10 @@
     for k in range(1, n_tp):
         copy_w(k).start()
     loads[4].wait()
+    xt[...] = x_ref[...].T.reshape(xt.shape)
+    for k in range(1, inner):
+        copy_x(k).start()
+    xg[:, lead, :, own_lanes] = xt[:, here, lead]
 
     value = nt(w_ref[...], x_ref[...]).astype(bf16)
     closing = cumulative[:, tokens - 1 : tokens]
@@ -230,10 +234,6 @@
     def of(a, h):
         return a[h * HEAD : (h + 1) * HEAD, :]
 
-    xt[...] = x_ref[...].T.reshape(xt.shape)
-    for k in range(1, inner):
-        copy_x(k).start()
-    xg[:, lead, :, own_lanes] = xt[:, here, lead]
     for h in range(heads):
         mixing = jnp.where(upper, tn(of(k_dec, h), of(q_dec, h)), 0.0).astype(bf16)
         gvk[here, h, 0] = nt(of(g, h), mixing).astype(bf16)
@@ -263,6 +263,16 @@
         lax.fori_loop(lo, hi, step, 0)
 
     each(outer - plane, outer, lambda k: copy_b2(k, plane).start())
+
+    pairing = [jnp.where(upper, tn(of(value, h), of(g, h)), 0.0).astype(bf16) for h in range(heads)]
+    gk_local = jnp.concatenate([nt(of(q_dec, h), pairing[h]) for h in range(heads)], axis=0)
+    gq_local = jnp.concatenate([nn(of(k_dec, h), pairing[h]) for h in range(heads)], axis=0)
+
+    for k in range(1, inner):
+        lanes = pl.ds(pl.multiple_of(source(k) * tokens, tokens), tokens)
+        rc(xt.at[:, 0, lead], xg.at[:, lead, :, lanes], x_send, x_recv, k, near(k)).wait_recv()
+    if part > 1:
+        copy_r(lead).start()
 
     for k in range(1, inner):
         copy_f1(k, source(k)).wait_recv()
@@ -279,16 +289,6 @@
     fmsg[0:packed, :] = running.astype(bf16)
     fmsg[packed : packed + LOGROWS, :] = plane_tail
     each(1, outer - plane, lambda k: copy_f2(k, plane).start())
-
-    pairing = [jnp.where(upper, tn(of(value, h), of(g, h)), 0.0).astype(bf16) for h in range(heads)]
-    gk_local = jnp.concatenate([nt(of(q_dec, h), pairing[h]) for h in range(heads)], axis=0)
-    gq_local = jnp.concatenate([nn(of(k_dec, h), pairing[h]) for h in range(heads)], axis=0)
-
-    for k in range(1, inner):
-        lanes = pl.ds(pl.multiple_of(source(k) * tokens, tokens), tokens)
-        rc(xt.at[:, 0, lead], xg.at[:, lead, :, lanes], x_send, x_recv, k, near(k)).wait_recv()
-    if part > 1:
-        copy_r(lead).start()
 
     empty = jnp.zeros((packed, wide), f32)
     none = [jnp.zeros((1, wide), f32) for _ in range(pairs + odd)]

time: 24.5 us -> 24.2 us (0.988)
  Pallas kernels: 23.7 us -> 23.4 us
    pallas_call x1, Pallas kernels: 22.9 us -> 22.6 us  [on_device(): pl.pallas_call(functools.partial(kernel, inner, outer, n_tp, part), out_s...]
where the time goes in v5:
time: 24.2 us; the launch traced here: 24.1 us
  Pallas kernels  23.4 us (97%)
  between operations  0.64 us (3%)
    pallas_call x1, Pallas kernels, on_device(): pl.pallas_call(functools.partial(kernel, inner, outer, n_tp, part), out_s...  22.6 us
    pallas_call x1, Pallas kernels, on_device(): pl.pallas_call(hand_on, out_shape=tuple((jax.ShapeDtypeStruct(a.shape, a....  0.8 us

profile of v5, /device:TPU:0, one launch (start us, length us, event | category | flops | bytes accessed | tf_op | source)
XLA Modules:
  0.0 24.1 jit_solution(9696147215593563152)
XLA Ops:
  0.6 22.6 %shard_map.93 = (bf16[192,128]{1,0:T(8,128)(2,1)S(1)}, bf16[192,128]{1,0:T(8,128)(2,1)S(1)}, bf16[64,2048]{1,0:T(8,128)(2,1)S(1)}, f32[192,128]{1,0:T(8,128)S(1)}) custom-call(bf16[128,2048]{1,0:T(8,128)(2,1)} %x_in.1, bf16[192,2048]{1,0:T(8,128)(2,1)} %bitcast.8, bf16[192,128]{1,0:T(8,128)(2,1)} %bitcast.9, bf16[192,128]{1,0:T(8,128)(2,1)} %bitcast.10, ...), custom_call_target="tpu_custom_call" | custom-call | tf_op jit(solution)/shard_map/pallas_call | solution.py:413
  23.3 0.8 %shard_map.94 = (bf16[192,128]{1,0:T(8,128)(2,1)}, bf16[192,128]{1,0:T(8,128)(2,1)}, bf16[64,2048]{1,0:T(8,128)(2,1)}, f32[192,128]{1,0:T(8,128)}) custom-call(bf16[192,128]{1,0:T(8,128)(2,1)S(1)} %get-tuple-element.12.refs_0_, bf16[192,128]{1,0:T(8,128)(2,1)S(1)} %get-tuple-element.13.refs_1_, bf16[64,2048]{1,0:T(8,128)(2,1)S(1)} %get-tuple-element.14.refs_2_, ...), custom_call_target="tpu_custom_call" | custom-call | tf_op jit(solution)/shard_map/pallas_call | solution.py:460
